TPU v7x, 32 devices: a whole 2x2x4 slice. The times are simulated.
32 devices in a mesh: tp: 16 (over z, y, x), dp: 2 (over core).
Axes of the slice: x: 2, y: 2, z: 4, core: 2. Of those that a mesh axis runs over, the one named last changes fastest.
Arguments:
- tokens: bfloat16 [256, 4096], P(None, 'dp'), may hold values from -20 to 20
- norm_gain: float32 [2, 4096], P(None, 'dp'), may hold values from 0.1 to 1.9
- receptance: bfloat16 [2, 4096, 1024], P(None, 'dp', 'tp'), may hold values from -0.09375 to 0.09375
- key_proj: bfloat16 [2, 4096, 1024], P(None, 'dp', 'tp'), may hold values from -0.09375 to 0.09375
- value_proj: bfloat16 [2, 4096, 1024], P(None, 'dp', 'tp'), may hold values from -0.09375 to 0.09375
- decay_proj: bfloat16 [2, 4096, 1024], P(None, 'dp', 'tp'), may hold values from -0.09375 to 0.09375
- rate_proj: bfloat16 [2, 4096, 1024], P(None, 'dp', 'tp'), may hold values from -0.09375 to 0.09375
- gate_proj: bfloat16 [2, 4096, 1024], P(None, 'dp', 'tp'), may hold values from -0.09375 to 0.09375
- decay_base: float32 [2, 1024], P(None, 'tp'), may hold values from -6 to 1
- group_gain: float32 [2, 1024], P(None, 'tp'), may hold values from 0.1 to 1.9
- output_proj: bfloat16 [2, 1024, 4096], P(None, 'tp', 'dp'), may hold values from -0.1875 to 0.1875
- state: float32 [2, 256, 16, 4096], P(None, 'dp', 'tp'), may hold values from -3 to 3
Outputs:
- next_tokens: bfloat16 [256, 4096], P(None, 'dp')
- new_state: float32 [2, 256, 16, 4096], P(None, 'dp', 'tp')
All inputs are finite; a program needn't handle non-finite values.
Results may differ from a plain program's by a relative error of at most 0.0066.
Values may be sent and summed in bfloat16 or wider, within the bound.
No kernel may reach another device: no remote copies, remote signals or barrier semaphores. Data moves between devices by JAX's collectives and lax.ppermute only.
A program may use at most 64 MiB of HBM per device.

v0:
```python
import jax
import jax.numpy as jnp
from jax import lax
from jax.sharding import PartitionSpec as P

D = 4096
HEAD = 64
LAYERS = 2
norm_floor = 0.1
group_floor = 0.5


def recurrence(state_block, recept_heads, key_heads, value_heads, decay_heads, rate_heads):
    log_rate = -jax.nn.softplus(-decay_heads) - 0.5
    forget = jnp.exp(-jnp.exp(log_rate))
    learn_rate = jax.nn.sigmoid(rate_heads)
    unit_key = key_heads * lax.rsqrt(jnp.sum(key_heads * key_heads, axis=-1, keepdims=True) + 1.0)
    scaled = key_heads * learn_rate
    removed = jnp.einsum("bhvk,bhk->bhv", state_block, -unit_key, precision=lax.Precision.HIGHEST)
    updated = (
        state_block * forget[:, :, None, :]
        + removed[..., None] * (unit_key * learn_rate)[:, :, None, :]
        + value_heads[..., None] * scaled[:, :, None, :]
    )
    read_out = jnp.einsum("bhvk,bhk->bhv", updated, recept_heads, precision=lax.Precision.HIGHEST)
    centre = read_out - jnp.mean(read_out, axis=-1, keepdims=True)
    normal = centre * lax.rsqrt(jnp.mean(centre * centre, axis=-1, keepdims=True) + group_floor)
    return (updated, normal)


def shards(
    tokens,
    norm_gain,
    receptance,
    key_proj,
    value_proj,
    decay_proj,
    rate_proj,
    gate_proj,
    decay_base,
    group_gain,
    output_proj,
    state,
):
    local_rows = state.shape[1]
    first_row = lax.axis_index("dp") * local_rows
    local_heads = state.shape[2]
    current = tokens
    finals = []
    for section_index in range(LAYERS):
        floats = current.astype(jnp.float32)
        squares = jnp.sum(floats * floats, axis=1)
        normed = (floats * norm_gain[section_index]).astype(jnp.bfloat16)
        part_recept = jnp.dot(normed, receptance[section_index], preferred_element_type=jnp.float32)
        part_key = jnp.dot(normed, key_proj[section_index], preferred_element_type=jnp.float32)
        part_value = jnp.dot(normed, value_proj[section_index], preferred_element_type=jnp.float32)
        part_decay = jnp.dot(normed, decay_proj[section_index], preferred_element_type=jnp.float32)
        part_rate = jnp.dot(normed, rate_proj[section_index], preferred_element_type=jnp.float32)
        part_gate = jnp.dot(normed, gate_proj[section_index], preferred_element_type=jnp.float32)
        totals = lax.psum(squares, "dp")
        own_squares = lax.dynamic_slice_in_dim(totals, first_row, local_rows, 0)
        summed = (
            lax.psum_scatter(part_recept, "dp", scatter_dimension=0, tiled=True),
            lax.psum_scatter(part_key, "dp", scatter_dimension=0, tiled=True),
            lax.psum_scatter(part_value, "dp", scatter_dimension=0, tiled=True),
            lax.psum_scatter(part_decay, "dp", scatter_dimension=0, tiled=True),
            lax.psum_scatter(part_rate, "dp", scatter_dimension=0, tiled=True),
            lax.psum_scatter(part_gate, "dp", scatter_dimension=0, tiled=True),
        )
        inv_rms = lax.rsqrt(own_squares / D + norm_floor)

        def by_head(term):
            rounded = lax.optimization_barrier((inv_rms[:, None] * term).astype(jnp.bfloat16))
            return rounded.astype(jnp.float32).reshape(local_rows, local_heads, HEAD)

        decay_heads = by_head(summed[3]) + decay_base[section_index].reshape(1, local_heads, HEAD)
        updated, normal = recurrence(
            state[section_index].reshape(local_rows, local_heads, HEAD, HEAD),
            by_head(summed[0]),
            by_head(summed[1]),
            by_head(summed[2]),
            decay_heads,
            by_head(summed[4]),
        )
        finals.append(updated.reshape(local_rows, local_heads, HEAD * HEAD))
        gate_value = jax.nn.sigmoid(by_head(summed[5]).reshape(local_rows, local_heads * HEAD))
        mixed_heads = (
            normal.reshape(local_rows, local_heads * HEAD) * group_gain[section_index] * gate_value
        ).astype(jnp.bfloat16)
        weights_out = output_proj[section_index]

        def apply_out(piece, begin, weights_out=weights_out):
            return jnp.dot(piece, weights_out, preferred_element_type=jnp.float32)

        partial_out = apply_out(lax.all_gather(mixed_heads, "dp", axis=0, tiled=True), jnp.int32(0))
        total = lax.psum(partial_out, "tp")
        current = (floats + total).astype(jnp.bfloat16)
    return (current, jnp.stack(finals))


def solution(mesh):
    return jax.shard_map(
        shards,
        mesh=mesh,
        in_specs=(
            P(None, "dp"),
            P(None, "dp"),
            P(None, "dp", "tp"),
            P(None, "dp", "tp"),
            P(None, "dp", "tp"),
            P(None, "dp", "tp"),
            P(None, "dp", "tp"),
            P(None, "dp", "tp"),
            P(None, "tp"),
            P(None, "tp"),
            P(None, "tp", "dp"),
            P(None, "dp", "tp", None),
        ),
        out_specs=(P(None, "dp"), P(None, "dp", "tp", None)),
        check_vma=False,
    )
```

profile of v0, /device:TPU:0, one launch (start us, length us, event | category | flops | bytes accessed | tf_op | source)
XLA Modules:
  0.0 421.7 jit_solution(14630838087907600654)
XLA Ops:
  8.1 2.3 fusion.22
  10.5 2.4 fusion.26
  17.6 8.1 %fusion.77 = (f32[1,128,1,4096]{3,2,1,0:T(1,128)}, f32[1,128,1,4096]{3,2,1,0:T(1,128)}) fusion(f32[2,128,1,4096]{3,2,1,0:T(1,128)} %param.23), kind=kLoop, calls=%fused_computation.119 | loop fusion | bytes 8388608 | tf_op jit(solution)/shard_map/slice | solution.py:78
  26.0 5.0 %copy.45 = f32[1,128,1,4096]{1,3,2,0:T(8,128)S(1)} copy(f32[1,128,1,4096]{3,2,1,0:T(1,128)} %get-tuple-element.7) | data formatting | bytes 4194304
  31.1 2.6 psum.28
  33.8 9.1 %reduce-scatter.17.cloned.1.call-done = f32[128,64]{0,1:T(8,128)} async-done(((f32[256,64]{0,1:T(8,128)}), f32[128,64]{0,1:T(8,128)}) %reduce-scatter.17.cloned.1.call-update) | async-done | bytes 32784 | tf_op jit(solution)/shard_map/reduce_scatter | solution.py:67
  42.8 10.7 %reduce-scatter.21.cloned.1.call-done = f32[128,64]{0,1:T(8,128)} async-done(((f32[256,64]{0,1:T(8,128)}), f32[128,64]{0,1:T(8,128)}) %reduce-scatter.21.cloned.1.call-update) | async-done | bytes 32784 | tf_op jit(solution)/shard_map/reduce_scatter | solution.py:63
  53.6 10.7 %reduce-scatter.23.cloned.1.call-done = f32[128,64]{0,1:T(8,128)} async-done(((f32[256,64]{0,1:T(8,128)}), f32[128,64]{0,1:T(8,128)}) %reduce-scatter.23.cloned.1.call-update) | async-done | bytes 32784 | tf_op jit(solution)/shard_map/reduce_scatter | solution.py:68
  64.3 10.7 %reduce-scatter.13.cloned.1.call-done = f32[128,64]{0,1:T(8,128)} async-done(((f32[256,64]{0,1:T(8,128)}), f32[128,64]{0,1:T(8,128)}) %reduce-scatter.13.cloned.1.call-update) | async-done | bytes 32784 | tf_op jit(solution)/shard_map/reduce_scatter | solution.py:66
  79.2 2.7 fusion.38
  82.0 5.6 %copy.46 = f32[1,128,1,4096]{1,3,2,0:T(8,128)} copy(f32[1,128,1,4096]{3,2,1,0:T(1,128)} %get-tuple-element.6) | data formatting | bytes 4194304
  87.7 122.2 %all-reduce.3.cloned.1.call-done = f32[256,2048]{1,0:T(8,128)} async-done(((f32[256,2048]{1,0:T(8,128)}), f32[256,2048]{1,0:T(8,128)}) %all-reduce.3.cloned.1.call-update) | async-done | bytes 2097168 | tf_op jit(solution)/shard_map/psum | solution.py:96
  214.0 2.4 fusion.14
  216.5 2.3 fusion.12
  225.2 2.6 broadcast_multiply_fusion.2
  227.8 2.6 psum.30
  231.9 10.7 %reduce-scatter.29.cloned.1.call-done = f32[128,64]{0,1:T(8,128)} async-done(((f32[256,64]{0,1:T(8,128)}), f32[128,64]{0,1:T(8,128)}) %reduce-scatter.29.cloned.1.call-update) | async-done | bytes 32784 | tf_op jit(solution)/shard_map/reduce_scatter | solution.py:67
  242.6 11.5 %reduce-scatter.33.cloned.1.call-done = f32[128,64]{0,1:T(8,128)} async-done(((f32[256,64]{0,1:T(8,128)}), f32[128,64]{0,1:T(8,128)}) %reduce-scatter.33.cloned.1.call-update) | async-done | bytes 32784 | tf_op jit(solution)/shard_map/reduce_scatter | solution.py:63
  254.1 10.7 %reduce-scatter.35.cloned.1.call-done = f32[128,64]{0,1:T(8,128)} async-done(((f32[256,64]{0,1:T(8,128)}), f32[128,64]{0,1:T(8,128)}) %reduce-scatter.35.cloned.1.call-update) | async-done | bytes 32784 | tf_op jit(solution)/shard_map/reduce_scatter | solution.py:68
  264.8 10.9 %reduce-scatter.25.cloned.1.call-done = f32[128,64]{0,1:T(8,128)} async-done(((f32[256,64]{0,1:T(8,128)}), f32[128,64]{0,1:T(8,128)}) %reduce-scatter.25.cloned.1.call-update) | async-done | bytes 32784 | tf_op jit(solution)/shard_map/reduce_scatter | solution.py:66
  281.7 2.7 fusion.30
  292.9 10.1 %copy.24 = f32[2,128,1,4096]{3,2,1,0:T(1,128)} copy(f32[2,128,1,4096]{1,3,2,0:T(8,128)} %pad_maximum_fusion) | data formatting | bytes 8388608
  303.1 109.3 %all-reduce.5.cloned.1.call-done = f32[256,2048]{1,0:T(8,128)} async-done(((f32[256,2048]{1,0:T(8,128)}), f32[256,2048]{1,0:T(8,128)}) %all-reduce.5.cloned.1.call-update) | async-done | bytes 2097168 | tf_op jit(solution)/shard_map/psum | solution.py:96
  412.4 2.8 fusion.5
  (109 shorter events, 36.4 us)
Async XLA Ops:
  7.2 5.8 %copy-start.3 = (bf16[256,2048]{1,0:T(8,128)(2,1)S(1)}, bf16[256,2048]{1,0:T(8,128)(2,1)}, u32[]{:S(2)}) copy-start(bf16[256,2048]{1,0:T(8,128)(2,1)} %param.12) | copy-start | bytes 3145732
  7.2 5.8 %copy-start.9 = (bf16[2,2048,64]{1,2,0:T(8,128)(2,1)S(1)}, bf16[2,2048,64]{1,2,0:T(8,128)(2,1)}, u32[]{:S(2)}) copy-start(bf16[2,2048,64]{1,2,0:T(8,128)(2,1)} %param.18) | copy-start | bytes 1572868
  7.2 26.6 %reduce-scatter.19.cloned.1.call-start = ((), (), s32[]{:S(2)}) async-start(), calls=%async_computation.15 | async-start | bytes 98304 | tf_op jit(solution)/shard_map/reduce_scatter | solution.py:65
  10.4 3.7 copy-start.10
  10.5 23.3 %reduce-scatter.15.cloned.1.call-start = ((), (), s32[]{:S(2)}) async-start(), calls=%async_computation.13 | async-start | bytes 98304 | tf_op jit(solution)/shard_map/reduce_scatter | solution.py:64
  12.9 2.4 copy-start.11
  12.9 29.9 %reduce-scatter.17.cloned.1.call-start = ((), (), s32[]{:S(2)}) async-start(), calls=%async_computation.14 | async-start | bytes 98304 | tf_op jit(solution)/shard_map/reduce_scatter | solution.py:67
  14.1 2.4 copy-start.12
  14.1 39.5 %reduce-scatter.21.cloned.1.call-start = ((), (), s32[]{:S(2)}) async-start(), calls=%async_computation.16 | async-start | bytes 98304 | tf_op jit(solution)/shard_map/reduce_scatter | solution.py:63
  15.2 49.1 %reduce-scatter.23.cloned.1.call-start = ((), (), s32[]{:S(2)}) async-start(), calls=%async_computation.17 | async-start | bytes 98304 | tf_op jit(solution)/shard_map/reduce_scatter | solution.py:68
  16.4 58.7 %reduce-scatter.13.cloned.1.call-start = ((), (), s32[]{:S(2)}) async-start(), calls=%async_computation.12 | async-start | bytes 98304 | tf_op jit(solution)/shard_map/reduce_scatter | solution.py:66
  17.5 8.2 %copy-start.6 = (f32[2,64]{1,0:T(2,128)S(1)}, f32[2,64]{1,0:T(2,128)}, u32[]{:S(2)}) copy-start(f32[2,64]{1,0:T(2,128)} %param.20) | copy-start | bytes 1540
  17.6 8.1 %copy-start.7 = (f32[2,64]{1,0:T(2,128)S(1)}, f32[2,64]{1,0:T(2,128)}, u32[]{:S(2)}) copy-start(f32[2,64]{1,0:T(2,128)} %param.21) | copy-start | bytes 1540
  17.6 192.3 %all-reduce.3.cloned.1.call-start = ((), (), s32[]{:S(2)}) async-start(), calls=%async_computation.18 | async-start | bytes 4194304 | tf_op jit(solution)/shard_map/psum | solution.py:96
  82.0 148.6 %reduce-scatter.31.cloned.1.call-start = ((), (), s32[]{:S(2)}) async-start(), calls=%async_computation.22 | async-start | bytes 98304 | tf_op jit(solution)/shard_map/reduce_scatter | solution.py:65
  209.9 3.0 copy-start.8
  214.0 5.0 %copy-start.5 = (bf16[256,2048]{1,0:T(8,128)(2,1)S(1)}, bf16[256,2048]{1,0:T(8,128)(2,1)}, u32[]{:S(2)}) copy-start(bf16[256,2048]{1,0:T(8,128)(2,1)} %copy-done.4) | copy-start | bytes 3145732
  214.0 17.9 %reduce-scatter.27.cloned.1.call-start = ((), (), s32[]{:S(2)}) async-start(), calls=%async_computation.20 | async-start | bytes 98304 | tf_op jit(solution)/shard_map/reduce_scatter | solution.py:64
  216.5 26.1 %reduce-scatter.29.cloned.1.call-start = ((), (), s32[]{:S(2)}) async-start(), calls=%async_computation.21 | async-start | bytes 98304 | tf_op jit(solution)/shard_map/reduce_scatter | solution.py:67
  218.9 35.2 %reduce-scatter.33.cloned.1.call-start = ((), (), s32[]{:S(2)}) async-start(), calls=%async_computation.23 | async-start | bytes 98304 | tf_op jit(solution)/shard_map/reduce_scatter | solution.py:63
  221.0 43.8 %reduce-scatter.35.cloned.1.call-start = ((), (), s32[]{:S(2)}) async-start(), calls=%async_computation.24 | async-start | bytes 98304 | tf_op jit(solution)/shard_map/reduce_scatter | solution.py:68
  223.1 52.6 %reduce-scatter.25.cloned.1.call-start = ((), (), s32[]{:S(2)}) async-start(), calls=%async_computation.19 | async-start | bytes 98304 | tf_op jit(solution)/shard_map/reduce_scatter | solution.py:66
  225.2 187.2 %all-reduce.5.cloned.1.call-start = ((), (), s32[]{:S(2)}) async-start(), calls=%async_computation.25 | async-start | bytes 4194304 | tf_op jit(solution)/shard_map/psum | solution.py:96
  275.7 3.2 copy-start
  (3 other events, 4.2 us)
Sparse Core Ops, SparseCore 0:
  10.8 10.2 reduce-scatter.18
  23.2 8.6 reduce-scatter.14
  34.2 8.6 reduce-scatter.16
  44.9 8.6 reduce-scatter.20
  55.6 8.6 reduce-scatter.22
  66.4 8.6 reduce-scatter.12
  82.1 127.7 all-reduce.2
  214.1 6.7 reduce-scatter.30
  223.1 8.7 reduce-scatter.26
  233.9 8.6 reduce-scatter.28
  245.4 8.6 reduce-scatter.32
  256.1 8.6 reduce-scatter.34
  267.0 8.6 reduce-scatter.24
  284.6 127.7 all-reduce.4
where the time goes:
time: 423 us; the launch traced here: 422 us
  waiting for transfers between devices  318 us (75%)
  local copies, waits for them, and re-layouts  33.9 us (8%)
  matrix products  26.4 us (6%)
  other arithmetic  19.5 us (5%)
  between operations  14.2 us (3%)
  blocking collectives  8.96 us (2%)
    psum x2, waiting for transfers between devices, shards(): total = lax.psum(partial_out, 'tp')  231 us
    unnamed x29, local copies, waits for them, and re-layouts  24.5 us
    reduce_scatter x2, waiting for transfers between devices, shards(): lax.psum_scatter(part_recept, 'dp', scatter_dimension=0, tiled=True)  22.2 us
    reduce_scatter x2, waiting for transfers between devices, shards(): lax.psum_scatter(part_decay, 'dp', scatter_dimension=0, tiled=True)  21.6 us
    reduce_scatter x2, waiting for transfers between devices, shards(): lax.psum_scatter(part_gate, 'dp', scatter_dimension=0, tiled=True)  21.5 us
    reduce_scatter x2, waiting for transfers between devices, shards(): lax.psum_scatter(part_rate, 'dp', scatter_dimension=0, tiled=True)  19.8 us
  transfers between devices with their start and end apart: 14, of which 11 were waited for; matrix products, arithmetic and copies ran while one was open for 13% of the time, Pallas kernels for 0%

commit v1 on v0

--- a/solution.py
+++ b/solution.py
@@ -93,7 +93,7 @@
             return jnp.dot(piece, weights_out, preferred_element_type=jnp.float32)
 
         partial_out = apply_out(lax.all_gather(mixed_heads, "dp", axis=0, tiled=True), jnp.int32(0))
-        total = lax.psum(partial_out, "tp")
+        total = jnp.sum(lax.all_gather(partial_out, "tp"), axis=0)
         current = (floats + total).astype(jnp.bfloat16)
     return (current, jnp.stack(finals))
 

time: 423 us -> 893 us (2.11)
  waiting for transfers between devices: 318 us -> 769 us
  other arithmetic: 19.5 us -> 39.2 us
    all_gather x0 -> x2, waiting for transfers between devices: none -> 687 us  [shards(): total = jnp.sum(lax.all_gather(partial_out, 'tp'), axis=0)]
    psum x2 -> x0, waiting for transfers between devices: 231 us -> none  [shards(): total = lax.psum(partial_out, 'tp')]
    reduce_sum x0 -> x2, other arithmetic: none -> 24.9 us  [shards(): total = jnp.sum(lax.all_gather(partial_out, 'tp'), axis=0)]
    reduce_scatter x2, waiting for transfers between devices: 0.01 us -> 22.8 us  [shards(): lax.psum_scatter(part_value, 'dp', scatter_dimension=0, tiled=True)]
    reduce_scatter x2, waiting for transfers between devices: 21.6 us -> 0.01 us  [shards(): lax.psum_scatter(part_decay, 'dp', scatter_dimension=0, tiled=True)]
    unnamed x29 -> x27, local copies, waits for them, and re-layouts: 24.5 us -> 23.4 us
  transfers between devices with their start and end apart: 14 -> 14, of which waited for: 11 -> 10; matrix products, arithmetic and copies ran while one was open for 13% -> 6% of each run, Pallas kernels for 0% -> 0%
where the time goes in v1:
time: 893 us; the launch traced here: 892 us
  waiting for transfers between devices  769 us (86%)
  other arithmetic  39.2 us (4%)
  local copies, waits for them, and re-layouts  32.8 us (4%)
  matrix products  26.3 us (3%)
  between operations  14.2 us (2%)
  blocking collectives  8.96 us (1%)
    all_gather x2, waiting for transfers between devices, shards(): total = jnp.sum(lax.all_gather(partial_out, 'tp'), axis=0)  687 us
    reduce_sum x2, other arithmetic, shards(): total = jnp.sum(lax.all_gather(partial_out, 'tp'), axis=0)  24.9 us
    unnamed x27, local copies, waits for them, and re-layouts  23.4 us
    reduce_scatter x2, waiting for transfers between devices, shards(): lax.psum_scatter(part_value, 'dp', scatter_dimension=0, tiled=True)  22.8 us
    reduce_scatter x2, waiting for transfers between devices, shards(): lax.psum_scatter(part_recept, 'dp', scatter_dimension=0, tiled=True)  21.6 us
    reduce_scatter x2, waiting for transfers between devices, shards(): lax.psum_scatter(part_gate, 'dp', scatter_dimension=0, tiled=True)  21.5 us
  transfers between devices with their start and end apart: 14, of which 10 were waited for; matrix products, arithmetic and copies ran while one was open for 6% of the time, Pallas kernels for 0%

profile of v1, /device:TPU:0, one launch (start us, length us, event | category | flops | bytes accessed | tf_op | source)
XLA Modules:
  0.0 891.5 jit_solution(6892970176508790689)
XLA Ops:
  8.1 2.3 fusion.28
  10.5 2.4 fusion.26
  17.6 8.1 fusion.77
  26.0 5.0 copy.45
  31.1 2.6 psum.14
  33.8 8.9 reduce-scatter.17.cloned.1.call-done
  42.6 11.3 %reduce-scatter.19.cloned.1.call-done = f32[128,64]{0,1:T(8,128)} async-done(((f32[256,64]{0,1:T(8,128)}), f32[128,64]{0,1:T(8,128)}) %reduce-scatter.19.cloned.1.call-update) | async-done | bytes 32784 | tf_op jit(solution)/shard_map/reduce_scatter | solution.py:65
  54.0 10.7 %reduce-scatter.21.cloned.1.call-done = f32[128,64]{0,1:T(8,128)} async-done(((f32[256,64]{0,1:T(8,128)}), f32[128,64]{0,1:T(8,128)}) %reduce-scatter.21.cloned.1.call-update) | async-done | bytes 32784 | tf_op jit(solution)/shard_map/reduce_scatter | solution.py:63
  64.7 10.7 %reduce-scatter.23.cloned.1.call-done = f32[128,64]{0,1:T(8,128)} async-done(((f32[256,64]{0,1:T(8,128)}), f32[128,64]{0,1:T(8,128)}) %reduce-scatter.23.cloned.1.call-update) | async-done | bytes 32784 | tf_op jit(solution)/shard_map/reduce_scatter | solution.py:68
  79.6 2.7 fusion.38
  82.4 351.5 %all-gather.5.cloned.1.call-done = f32[4096,2048]{1,0:T(8,128)} async-done(((f32[256,2048]{1,0:T(8,128)}), f32[4096,2048]{1,0:T(8,128)}) %all-gather.5.cloned.1.call-update) | async-done | bytes 33554448 | tf_op jit(solution)/shard_map/all_gather | solution.py:96
  433.9 13.1 %reduce_sum.94 = f32[256,2048]{1,0:T(8,128)} reduce(f32[16,256,2048]{2,1,0:T(8,128)} %bitcast.73, f32[]{:T(128)} %constant.11.clone.1), dimensions={0}, to_apply=%region_11.12 | reduce | flops 7864320 | bytes 35651588 | tf_op jit(solution)/shard_map/reduce_sum | solution.py:96
  451.1 2.4 fusion.14
  453.6 2.3 fusion.12
  462.3 5.6 copy.46
  468.0 2.6 psum.15
  470.7 7.9 reduce-scatter.29.cloned.1.call-done
  478.6 10.9 %reduce-scatter.33.cloned.1.call-done = f32[128,64]{0,1:T(8,128)} async-done(((f32[256,64]{0,1:T(8,128)}), f32[128,64]{0,1:T(8,128)}) %reduce-scatter.33.cloned.1.call-update) | async-done | bytes 32784 | tf_op jit(solution)/shard_map/reduce_scatter | solution.py:63
  489.5 10.7 %reduce-scatter.35.cloned.1.call-done = f32[128,64]{0,1:T(8,128)} async-done(((f32[256,64]{0,1:T(8,128)}), f32[128,64]{0,1:T(8,128)}) %reduce-scatter.35.cloned.1.call-update) | async-done | bytes 32784 | tf_op jit(solution)/shard_map/reduce_scatter | solution.py:68
  500.2 11.5 %reduce-scatter.31.cloned.1.call-done = f32[128,64]{0,1:T(8,128)} async-done(((f32[256,64]{0,1:T(8,128)}), f32[128,64]{0,1:T(8,128)}) %reduce-scatter.31.cloned.1.call-update) | async-done | bytes 32784 | tf_op jit(solution)/shard_map/reduce_scatter | solution.py:65
  517.6 2.7 fusion.30
  526.5 10.4 %copy.24 = f32[2,128,1,4096]{3,2,1,0:T(1,128)} copy(f32[2,128,1,4096]{1,3,2,0:T(8,128)} %pad_maximum_fusion) | data formatting | bytes 8388608
  536.9 335.1 %all-gather.7.cloned.1.call-done = f32[4096,2048]{1,0:T(8,128)} async-done(((f32[256,2048]{1,0:T(8,128)}), f32[4096,2048]{1,0:T(8,128)}) %all-gather.7.cloned.1.call-update) | async-done | bytes 33554448 | tf_op jit(solution)/shard_map/all_gather | solution.py:96
  871.9 11.8 %reduce_sum.99 = f32[256,2048]{1,0:T(8,128)S(1)} reduce(f32[16,256,2048]{2,1,0:T(8,128)} %bitcast.72, f32[]{:T(128)} %constant.11.clone.1), dimensions={0}, to_apply=%region_23.24 | reduce | flops 7864320 | bytes 35651588 | tf_op jit(solution)/shard_map/reduce_sum | solution.py:96
  (109 shorter events, 33.9 us)
Async XLA Ops:
  7.2 5.8 copy-start.2
  7.2 5.8 copy-start.8
  7.2 26.6 %reduce-scatter.13.cloned.1.call-start = ((), (), s32[]{:S(2)}) async-start(), calls=%async_computation.12 | async-start | bytes 98304 | tf_op jit(solution)/shard_map/reduce_scatter | solution.py:66
  10.4 3.7 copy-start.11
  10.5 23.3 %reduce-scatter.15.cloned.1.call-start = ((), (), s32[]{:S(2)}) async-start(), calls=%async_computation.13 | async-start | bytes 98304 | tf_op jit(solution)/shard_map/reduce_scatter | solution.py:64
  12.9 2.4 copy-start.9
  12.9 29.7 %reduce-scatter.17.cloned.1.call-start = ((), (), s32[]{:S(2)}) async-start(), calls=%async_computation.14 | async-start | bytes 98304 | tf_op jit(solution)/shard_map/reduce_scatter | solution.py:67
  14.0 2.4 copy-start.10
  14.1 39.9 %reduce-scatter.19.cloned.1.call-start = ((), (), s32[]{:S(2)}) async-start(), calls=%async_computation.15 | async-start | bytes 98304 | tf_op jit(solution)/shard_map/reduce_scatter | solution.py:65
  15.2 49.4 %reduce-scatter.21.cloned.1.call-start = ((), (), s32[]{:S(2)}) async-start(), calls=%async_computation.16 | async-start | bytes 98304 | tf_op jit(solution)/shard_map/reduce_scatter | solution.py:63
  16.4 59.0 %reduce-scatter.23.cloned.1.call-start = ((), (), s32[]{:S(2)}) async-start(), calls=%async_computation.17 | async-start | bytes 98304 | tf_op jit(solution)/shard_map/reduce_scatter | solution.py:68
  17.5 8.2 copy-start.5
  17.6 8.2 copy-start.6
  17.6 416.3 %all-gather.5.cloned.1.call-start = ((), (), s32[]{:S(2)}) async-start(), calls=%async_computation.24 | async-start | bytes 35651584 | tf_op jit(solution)/shard_map/all_gather | solution.py:96
  82.3 388.4 %reduce-scatter.25.cloned.1.call-start = ((), (), s32[]{:S(2)}) async-start(), calls=%async_computation.18 | async-start | bytes 98304 | tf_op jit(solution)/shard_map/reduce_scatter | solution.py:66
  447.0 3.0 copy-start.7
  451.1 5.0 copy-start.4
  451.1 19.6 %reduce-scatter.27.cloned.1.call-start = ((), (), s32[]{:S(2)}) async-start(), calls=%async_computation.19 | async-start | bytes 98304 | tf_op jit(solution)/shard_map/reduce_scatter | solution.py:64
  453.6 25.0 %reduce-scatter.29.cloned.1.call-start = ((), (), s32[]{:S(2)}) async-start(), calls=%async_computation.20 | async-start | bytes 98304 | tf_op jit(solution)/shard_map/reduce_scatter | solution.py:67
  456.0 33.5 %reduce-scatter.33.cloned.1.call-start = ((), (), s32[]{:S(2)}) async-start(), calls=%async_computation.22 | async-start | bytes 98304 | tf_op jit(solution)/shard_map/reduce_scatter | solution.py:63
  458.1 42.1 %reduce-scatter.35.cloned.1.call-start = ((), (), s32[]{:S(2)}) async-start(), calls=%async_computation.23 | async-start | bytes 98304 | tf_op jit(solution)/shard_map/reduce_scatter | solution.py:68
  460.2 51.5 %reduce-scatter.31.cloned.1.call-start = ((), (), s32[]{:S(2)}) async-start(), calls=%async_computation.21 | async-start | bytes 98304 | tf_op jit(solution)/shard_map/reduce_scatter | solution.py:65
  462.3 409.6 %all-gather.7.cloned.1.call-start = ((), (), s32[]{:S(2)}) async-start(), calls=%async_computation.25 | async-start | bytes 35651584 | tf_op jit(solution)/shard_map/all_gather | solution.py:96
  511.7 3.2 copy-start
  (2 other events, 2.6 us)
Sparse Core Ops, SparseCore 0:
  10.6 10.2 reduce-scatter.12
  23.1 8.6 reduce-scatter.14
  33.9 8.6 reduce-scatter.16
  45.3 8.6 reduce-scatter.18
  56.0 8.6 reduce-scatter.20
  66.7 8.6 reduce-scatter.22
  82.4 351.3 all-gather.4
  451.2 5.7 reduce-scatter.24
  459.2 8.6 reduce-scatter.26
  469.9 8.6 reduce-scatter.28
  480.8 8.6 reduce-scatter.32
  491.5 8.6 reduce-scatter.34
  503.0 8.6 reduce-scatter.30
  520.5 351.3 all-gather.6
